TPU v7x, 32 devices: a whole 2x2x4 slice. The times are simulated.
32 devices in a mesh: kv: 8 (over z, x), tp: 4 (over y, core).
Axes of the slice: x: 2, y: 2, z: 4, core: 2. Of those that a mesh axis runs over, the one named last changes fastest.
Arguments:
- activations: bfloat16 [384, 2048], P(None, ('kv', 'tp')), may hold values from -6 to 6
- latent_cache: bfloat16 [24, 16384, 288], P(None, 'kv'), may hold values from -6 to 6
- lengths: int32 [24], replicated, may hold values from 4096 to 16352, as said below
- accepted: int32 [24], replicated, may hold values from 0 to 16
- parents: int32 [24, 16], replicated, may hold values from -1 to 14, as said below
- w_query_down: bfloat16 [2048, 512], P(('kv', 'tp')), may hold values from -0.125 to 0.125
- w_key_down: bfloat16 [2048, 288], P(('kv', 'tp')), may hold values from -0.125 to 0.125
- gain_input: bfloat16 [2048], P(('kv', 'tp')), may hold values from 0.099609375 to 1.8984375
- gain_query: bfloat16 [512], replicated, may hold values from 0.099609375 to 1.8984375
- gain_key: bfloat16 [256], replicated, may hold values from 0.099609375 to 1.8984375
- w_query: bfloat16 [512, 16, 288], P(None, 'tp'), as said below
- w_value: bfloat16 [16, 256, 64], replicated, may hold values from -0.375 to 0.375
- w_out: bfloat16 [1024, 2048], P('tp', 'kv'), may hold values from -1 to 1, as said below
- gain_output: bfloat16 [2048], P('kv'), may hold values from 0.099609375 to 1.8984375
Outputs:
- mixed: bfloat16 [384, 2048], P(None, 'kv')
- new_cache: bfloat16 [24, 16384, 288], P(None, 'kv')
Inputs may be any that keep to these rules, and one draw needn't show every extreme that they name: One sequence has lengths exactly 16352 and another exactly 4096; which ones varies. accepted is between 0 and 16, so the proposals' positions lie below 16384. `parents`: the parent of proposal i is -1 or a proposal with a smaller index; proposal 0 has parent -1; the proposals of exactly one sequence (which one varies) form a single chain; the other sequences' proposals form general trees. `w_query`: entries are normal with standard deviation (1536)^(-1/2) cut at six standard deviations; in the hidden draw the heads whose index is a multiple of 4 are 48 times larger. `w_out`: entries of order (1024)^(-1/2).
All inputs are finite; a program needn't handle non-finite values.
Results may differ from a plain program's by a relative error of at most 0.0096.
The roundings to bfloat16 on the way count: a program that leaves them out, or rounds other values in their place, can miss the bound.
Values may be sent and summed in bfloat16 or wider, within the bound.
A program may use at most 192 MiB of HBM per device.

v0:
```python
import jax
import jax.numpy as jnp
from jax import lax
from jax.sharding import PartitionSpec as P

D = 2048
ROPE_DIM = 32
NOPE_DIM = 64
epsilon = 1e-06
rope_base = 10000.0
score_after_mask = -1e30


def rotate(component, places):
    half_width = component.shape[-1] // 2
    frequency = rope_base ** (-jnp.arange(half_width, dtype=jnp.float32) / half_width)
    angles = places.astype(jnp.float32)[:, None] * frequency[None, :]
    target_shape = (places.shape[0],) + (1,) * (component.ndim - 2) + (half_width,)
    cosine = jnp.cos(angles).reshape(target_shape)
    sine_part = jnp.sin(angles).reshape(target_shape)
    front_half = component[..., :half_width]
    back_half = component[..., half_width:]
    return jnp.concatenate(
        [front_half * cosine - back_half * sine_part, back_half * cosine + front_half * sine_part],
        axis=-1,
    )


def normalize(values, scales):
    return (
        values
        * lax.rsqrt(jnp.mean(values * values, axis=-1, keepdims=True) + epsilon)
        * scales.astype(jnp.float32)
    )


def ancestry(parents):
    seq_count, prop_count = parents.shape
    slot_ids = jnp.arange(prop_count, dtype=jnp.int32)
    parent_links = (parents[:, :, None] == slot_ids[None, None, :]).astype(jnp.float32)
    identity = jnp.broadcast_to(jnp.eye(prop_count, dtype=jnp.float32), parent_links.shape)
    reached = jnp.minimum(identity + parent_links, 1.0)
    for repeat in range((prop_count - 1).bit_length()):
        reached = jnp.minimum(
            jnp.einsum("sij,sjk->sik", reached, reached, precision=lax.Precision.HIGHEST), 1.0
        )
    depths = (jnp.sum(reached, axis=-1) - 1.0).astype(jnp.int32)
    return (reached, depths)


def down_terms(features, gain_rows, query_down, key_down):
    as_float = features.astype(jnp.float32)
    scaled = (as_float * gain_rows.astype(jnp.float32)).astype(jnp.bfloat16)
    squares = jnp.sum(as_float * as_float, axis=-1)
    query_segment = jnp.dot(scaled, query_down, preferred_element_type=jnp.float32)
    key_segment = jnp.dot(scaled, key_down, preferred_element_type=jnp.float32)
    return (squares, query_segment, key_segment)


def partial_attend(queries, key_rows, slot_index, onehot, reached, kv_rank, value_locally):
    score_scale = (NOPE_DIM + ROPE_DIM) ** (-0.5)
    ancestors = jnp.einsum("sij,snj->sin", reached, onehot, precision=lax.Precision.HIGHEST)
    visible = ((slot_index < 0)[:, None, :] | (ancestors > 0.5))[:, :, None, :]
    scores = (
        jnp.einsum("siha,sna->sihn", queries, key_rows, preferred_element_type=jnp.float32)
        * score_scale
    )
    masked = jnp.where(visible, scores, score_after_mask)
    maxima = jnp.max(masked, axis=-1)
    weights = jnp.where(visible, jnp.exp(masked - maxima[..., None]), 0.0)
    totals = jnp.sum(weights, axis=-1)
    weighted = jnp.einsum(
        "sihn,snk->sihk",
        weights.astype(jnp.bfloat16),
        key_rows[:, :, :kv_rank],
        preferred_element_type=jnp.float32,
    )
    value_fraction = (weighted / jnp.maximum(totals, 1.0)[..., None]).astype(jnp.bfloat16)
    values = jnp.einsum(
        "pwmb,mbe->pwme", value_fraction, value_locally, preferred_element_type=jnp.float32
    )
    return (maxima, totals, values.astype(jnp.bfloat16))


def combine_parts(maxima, totals, values):
    largest = jnp.max(maxima, axis=0)
    shares = totals * jnp.exp(maxima - largest[None])
    summed = jnp.sum(shares[..., None] * values.astype(jnp.float32), axis=0)
    return (summed / jnp.sum(shares, axis=0)[..., None]).astype(jnp.bfloat16)


def local(
    activations,
    latent_cache,
    lengths,
    accepted,
    parents,
    w_query_down,
    w_key_down,
    gain_input,
    gain_query,
    gain_key,
    w_query,
    w_value,
    w_out,
    gain_output,
):
    seq_count, prop_count = parents.shape
    row_count = activations.shape[0]
    heads_here = w_query.shape[1]
    kv_rank = gain_key.shape[0]
    span_len = latent_cache.shape[1]
    reached, depths = ancestry(parents)
    filled = lengths + accepted
    places = (filled[:, None] + depths).reshape(-1)
    features, gain_rows, query_down, key_down = (
        lax.all_gather(activations, "tp", axis=1, tiled=True),
        lax.all_gather(gain_input, "tp", axis=0, tiled=True),
        lax.all_gather(w_query_down, "tp", axis=0, tiled=True),
        lax.all_gather(w_key_down, "tp", axis=0, tiled=True),
    )
    squares, query_segment, key_segment = down_terms(features, gain_rows, query_down, key_down)
    squares, query_raw, key_raw = lax.psum((squares, query_segment, key_segment), "kv")
    inverse = lax.rsqrt(squares / D + epsilon)[:, None]
    query_low = normalize(query_raw * inverse, gain_query).astype(jnp.bfloat16)
    key_full = key_raw * inverse
    mapped_output = jnp.dot(
        query_low, w_query.reshape(w_query.shape[0], -1), preferred_element_type=jnp.float32
    )
    mapped_output = mapped_output.reshape(row_count, heads_here, -1)
    queries = jnp.concatenate(
        [mapped_output[..., :kv_rank], rotate(mapped_output[..., kv_rank:], places)], axis=-1
    ).astype(jnp.bfloat16)
    fresh_rows = jnp.concatenate(
        [normalize(key_full[:, :kv_rank], gain_key), rotate(key_full[:, kv_rank:], places)], axis=-1
    ).astype(jnp.bfloat16)
    locations_held = lax.axis_index("kv") * span_len + jnp.arange(span_len, dtype=jnp.int32)
    slot_index = locations_held[None, :] - filled[:, None]
    onehot = slot_index[:, :, None] == jnp.arange(prop_count, dtype=jnp.int32)[None, None, :]
    fresh_block = fresh_rows.reshape(seq_count, prop_count, -1)
    placed = jnp.einsum(
        "snj,sja->sna", onehot.astype(jnp.bfloat16), fresh_block, preferred_element_type=jnp.float32
    ).astype(jnp.bfloat16)
    updated = jnp.where(jnp.any(onehot, axis=-1)[:, :, None], placed, latent_cache)
    head_start = lax.axis_index("tp") * heads_here
    value_locally = lax.dynamic_slice_in_dim(w_value, head_start, heads_here, 0)
    maxima, totals, values = partial_attend(
        queries.reshape(seq_count, prop_count, heads_here, -1),
        updated,
        slot_index,
        onehot.astype(jnp.float32),
        reached,
        kv_rank,
        value_locally,
    )
    maxima = maxima.reshape(1, row_count, heads_here)
    totals = totals.reshape(1, row_count, heads_here)
    values = values.reshape(1, row_count, heads_here, -1)
    maxima, totals = (
        lax.all_gather(maxima, "kv", axis=0, tiled=True),
        lax.all_gather(totals, "kv", axis=0, tiled=True),
    )
    values = lax.all_gather(values, "kv", axis=0, tiled=True)
    attended = combine_parts(maxima, totals, values).reshape(row_count, -1)
    head_terms = jnp.dot(attended, w_out, preferred_element_type=jnp.float32)
    mixed_raw = lax.psum(head_terms, "tp")
    total_sq = lax.psum(jnp.sum(mixed_raw * mixed_raw, axis=-1), "kv")
    result = (
        mixed_raw * lax.rsqrt(total_sq / D + epsilon)[:, None] * gain_output.astype(jnp.float32)
    ).astype(jnp.bfloat16)
    return (result, updated)


def solution(mesh):
    in_specs = (
        P(None, ("kv", "tp")),
        P(None, "kv", None),
        P(),
        P(),
        P(),
        P(("kv", "tp"), None),
        P(("kv", "tp"), None),
        P(("kv", "tp")),
        P(),
        P(),
        P(None, "tp", None),
        P(),
        P("tp", "kv"),
        P("kv"),
    )
    out_specs = (P(None, "kv"), P(None, "kv", None))
    return jax.shard_map(local, mesh=mesh, in_specs=in_specs, out_specs=out_specs, check_vma=False)
```

profile of v0, /device:TPU:0, one launch (start us, length us, event | category | flops | bytes accessed | tf_op | source)
XLA Modules:
  0.0 322.6 jit_solution(7853236697493390630)
XLA Ops:
  7.2 1.3 dynamic-slice
  9.2 0.9 dynamic-update-slice
  10.1 8.4 %all-reduce = bf16[256]{0:T(256)(128)(2,1)S(1)} all-reduce(bf16[256]{0:T(256)(128)(2,1)S(1)} %dynamic-update-slice), channel_id=1, replica_groups=mesh['kv'=8,'tp'=4] {'tp'}, use_global_device_ids=true, to_apply=%add | all-reduce | flops 256 | bytes 1024
  18.5 5.8 %all_gather.21 = bf16[384,256]{0,1:T(8,128)(2,1)S(1)} all-gather(bf16[384,64]{0,1:T(8,128)(2,1)} %param.14), channel_id=1, replica_groups=mesh['kv'=8,'tp'=4] {'tp'}, dimensions={1}, use_global_device_ids=true | all-gather | bytes 245760 | tf_op jit(solution)/shard_map/all_gather | solution.py:117
  24.3 6.0 %all_gather.23 = bf16[256,512]{1,0:T(8,128)(2,1)S(1)} all-gather(bf16[64,512]{1,0:T(8,128)(2,1)} %param.19), channel_id=1, replica_groups=mesh['kv'=8,'tp'=4] {'tp'}, dimensions={0}, use_global_device_ids=true | all-gather | bytes 327680 | tf_op jit(solution)/shard_map/all_gather | solution.py:119
  30.3 5.8 %all_gather.24 = bf16[256,288]{1,0:T(8,128)(2,1)S(1)} all-gather(bf16[64,288]{1,0:T(8,128)(2,1)} %param.20), channel_id=1, replica_groups=mesh['kv'=8,'tp'=4] {'tp'}, dimensions={0}, use_global_device_ids=true | all-gather | bytes 184320 | tf_op jit(solution)/shard_map/all_gather | solution.py:120
  36.1 1.3 fusion.49
  37.4 1.1 fusion.47
  38.6 22.2 %psum.36 = f32[384]{0:T(512)S(1)} all-reduce(f32[384]{0:T(512)S(1)} %fusion.28), channel_id=1, replica_groups=mesh['kv'=8,'tp'=4] {'kv'}, use_global_device_ids=true, to_apply=%region_2.0 | all-reduce | flops 384 | bytes 3072 | tf_op jit(solution)/shard_map/psum | solution.py:123
  61.5 0.8 copy.38
  65.4 1.5 fusion.12
  67.0 2.0 compare_or_fusion
  69.1 51.6 %all-reduce.7.cloned.1.call-done = (f32[384,288]{0,1:T(8,128)}, f32[384,512]{1,0:T(8,128)}) async-done(((f32[384,288]{0,1:T(8,128)}, f32[384,512]{1,0:T(8,128)}), (f32[384,288]{0,1:T(8,128)}, f32[384,512]{1,0:T(8,128)})) %all-reduce.7.cloned.1.call-update) | async-done | bytes 1228816 | tf_op jit(solution)/shard_map/psum | solution.py:123
  120.7 1.0 broadcast_multiply_fusion
  122.2 0.7 copy.61
  123.0 0.7 copy.62
  123.7 1.4 multiply_reduce_fusion.1
  125.1 2.0 fusion.22
  128.9 25.2 %convert_select_fusion = bf16[24,2048,288]{1,2,0:T(8,128)(2,1)} fusion(bf16[24,2048,288]{1,2,0:T(8,128)(2,1)} %param.15, pred[24,2048]{1,0:T(8,128)(4,1)} %fusion.12, s32[24,2048]{1,0:T(8,128)S(1)} %broadcast_subtract_fusion, bf16[24,16,16]{2,1,0:T(8,128)(2,1)} %bitcast.62, bf16[24,16,16]{2,1,0:T(8,128)(2,1)} %bitcast.61, bf16[24,16,256]{2,1,0:T(8,128)(2,1)S(1)} %bitcast.60), kind=kOutput, calls=%fused_computation.2 | convolution fusion | flops 482746368 | bytes 57090048 | tf_op jit(solution)/shard_map/snj,sja->sna/dot_general | solution.py:141
  154.1 15.5 %fusion.3 = (f32[24,16,4]{1,2,0:T(4,128)S(1)}, f32[24,16,4,2048]{3,1,2,0:T(8,128)}) fusion(pred[24,16,2048]{2,1,0:T(8,128)(4,1)S(1)} %compare_or_fusion, bf16[24,2048,288]{1,2,0:T(8,128)(2,1)} %convert_select_fusion, bf16[24,16,4,16]{3,1,2,0:T(8,128)(2,1)S(1)} %copy.44, bf16[24,16,4,16]{3,1,2,0:T(8,128)(2,1)S(1)} %copy.43, ...), kind=kOutput, calls=%fused_computation.7 | convolution fusion | flops 1824029184 | bytes 42571776 | tf_op jit(solution)/shard_map/siha,sna->sihn/dot_general | solution.py:65
  169.6 6.9 %fusion.5 = f32[24,16,4]{1,2,0:T(4,128)S(1)} fusion(f32[24,16,4,2048]{3,1,2,0:T(8,128)} %get-tuple-element.17, f32[24,16,4]{1,2,0:T(4,128)S(1)} %get-tuple-element.16, pred[24,16,2048]{2,1,0:T(8,128)(4,1)S(1)} %compare_or_fusion), kind=kLoop, calls=%fused_computation.9 | loop fusion | flops 15727104 | bytes 13381632 | tf_op jit(solution)/shard_map/reduce_sum | solution.py:71
  176.5 15.1 %divide_convert_fusion = bf16[24,16,4,256]{3,1,2,0:T(8,128)(2,1)S(1)} fusion(bf16[24,2048,288]{1,2,0:T(8,128)(2,1)} %convert_select_fusion, f32[24,16,4,2048]{3,1,2,0:T(8,128)} %get-tuple-element.17, f32[24,16,4]{1,2,0:T(4,128)S(1)} %get-tuple-element.16, pred[24,16,2048]{2,1,0:T(8,128)(4,1)S(1)} %compare_or_fusion, f32[24,16,4]{1,2,0:T(4,128)S(1)} %broadcast_maximum_fusion), kind=kOutput, calls=%fused_computation.21 | convolution fusion | flops 1627127808 | bytes 39333888 | tf_op jit(solution)/shard_map/sihn,snk->sihk/dot_general | solution.py:72
  191.7 1.6 fusion.16
  193.4 0.8 copy.53
  194.5 30.7 %all_gather.26 = f32[8,384,4]{1,2,0:T(4,128)S(1)} all-gather(f32[1,384,4]{1,2,0:T(4,128)S(1)} %reshape.200), channel_id=1, replica_groups=mesh['kv'=8,'tp'=4] {'kv'}, dimensions={0}, use_global_device_ids=true | all-gather | bytes 55296 | tf_op jit(solution)/shard_map/all_gather | solution.py:160
  225.3 30.9 %all_gather.25 = f32[8,384,4]{1,2,0:T(4,128)S(1)} all-gather(f32[1,384,4]{1,2,0:T(4,128)S(1)} %reshape.199), channel_id=1, replica_groups=mesh['kv'=8,'tp'=4] {'kv'}, dimensions={0}, use_global_device_ids=true | all-gather | bytes 55296 | tf_op jit(solution)/shard_map/all_gather | solution.py:161
  256.2 1.8 multiply_reduce_fusion
  258.7 1.0 fusion.61
  259.8 32.0 %all-reduce.5.cloned.1.call-done = f32[384,256]{1,0:T(8,128)} async-done(((f32[384,256]{1,0:T(8,128)}), f32[384,256]{1,0:T(8,128)}) %all-reduce.5.cloned.1.call-update) | async-done | bytes 393232 | tf_op jit(solution)/shard_map/psum | solution.py:166
  291.7 1.1 multiply_reduce_fusion.2
  292.9 21.4 %psum.39 = f32[384]{0:T(512)S(1)} all-reduce(f32[384]{0:T(512)S(1)} %multiply_reduce_fusion.2), channel_id=1, replica_groups=mesh['kv'=8,'tp'=4] {'kv'}, use_global_device_ids=true, to_apply=%region_15.16 | all-reduce | flops 384 | bytes 3072 | tf_op jit(solution)/shard_map/psum | solution.py:167
  314.2 1.8 multiply_convert_fusion.1
  (59 shorter events, 7.4 us)
Async XLA Ops:
  7.2 117.9 %copy-start = (bf16[512,4,288]{0,2,1:T(8,128)(2,1)S(1)}, bf16[512,4,288]{0,2,1:T(8,128)(2,1)}, u32[]{:S(2)}) copy-start(bf16[512,4,288]{0,2,1:T(8,128)(2,1)} %param.24) | copy-start | bytes 3538948
  7.2 113.5 %all-reduce.7.cloned.1.call-start = ((), (), s32[]{:S(2)}) async-start(), calls=%async_computation.2 | async-start | bytes 2457600 | tf_op jit(solution)/shard_map/psum | solution.py:123
  38.5 217.7 %all-gather.2.cloned.1.call-start = ((), (), s32[]{:S(2)}) async-start(), calls=%async_computation | async-start | bytes 1769472 | tf_op jit(solution)/shard_map/all_gather | solution.py:163
  176.5 82.2 %copy-start.2 = (bf16[256,256]{1,0:T(8,128)(2,1)S(1)}, bf16[256,256]{1,0:T(8,128)(2,1)}, u32[]{:S(2)}) copy-start(bf16[256,256]{1,0:T(8,128)(2,1)} %param.26) | copy-start | bytes 393220
  176.5 83.2 %copy-start.3 = (bf16[256]{0:T(256)(128)(2,1)S(1)}, bf16[256]{0:T(256)(128)(2,1)}, u32[]{:S(2)}) copy-start(bf16[256]{0:T(256)(128)(2,1)} %param.27) | copy-start | bytes 1540
  176.5 139.5 %copy-start.1 = (bf16[512,4,288]{0,2,1:T(8,128)(2,1)S(1)}, bf16[512,4,288]{0,2,1:T(8,128)(2,1)}, u32[]{:S(2)}) copy-start(bf16[512,4,288]{0,2,1:T(8,128)(2,1)} %param.24) | copy-start | bytes 3538948
  194.2 97.5 %all-reduce.5.cloned.1.call-start = ((), (), s32[]{:S(2)}) async-start(), calls=%async_computation.1 | async-start | bytes 786432 | tf_op jit(solution)/shard_map/psum | solution.py:166
Sparse Core Ops, SparseCore 0:
  38.6 81.9 all-reduce.6
  194.4 43.4 all-gather.1
  259.9 31.8 all-reduce.4
where the time goes:
time: 323 us
  blocking collectives  131 us (41%)
  waiting for transfers between devices  83.6 us (26%)
  matrix products  66.4 us (21%)
  other arithmetic  18.6 us (6%)
  between operations  14.7 us (5%)
  local copies, waits for them, and re-layouts  7.89 us (2%)
    psum x1, waiting for transfers between devices, local(): lax.psum((squares, query_segment, key_segment), 'kv')  51.6 us
    psum x1, waiting for transfers between devices, local(): mixed_raw = lax.psum(head_terms, 'tp')  32 us
    all_gather x1, blocking collectives, local(): lax.all_gather(totals, 'kv', axis=0, tiled=True)  30.9 us
    all_gather x1, blocking collectives, local(): lax.all_gather(maxima, 'kv', axis=0, tiled=True)  30.7 us
    dot_general x1, matrix products, local(): jnp.einsum('snj,sja->sna', onehot.astype(jnp.bfloat16), fresh_block, pref...  25.2 us
    psum x1, blocking collectives, local(): lax.psum((squares, query_segment, key_segment), 'kv')  22.2 us
    psum x1, blocking collectives, local(): total_sq = lax.psum(jnp.sum(mixed_raw * mixed_raw, axis=-1), 'kv')  21.4 us
    dot_general x1, matrix products, partial_attend(): jnp.einsum('siha,sna->sihn', queries, key_rows, preferred_element_type=jn...  15.5 us
  transfers between devices with their start and end apart: 3, of which 2 were waited for; matrix products, arithmetic and copies ran while one was open for 3% of the time, Pallas kernels for 0%

commit v1 on v0

--- a/solution.py
+++ b/solution.py
@@ -157,7 +157,9 @@
     totals = totals.reshape(1, row_count, heads_here)
     values = values.reshape(1, row_count, heads_here, -1)
     maxima, totals = (
-        lax.all_gather(maxima, "kv", axis=0, tiled=True),
+        jnp.concatenate(
+            lax.all_to_all(jnp.stack([maxima] * lax.axis_size("kv")), "kv", 0, 0), axis=0
+        ),
         lax.all_gather(totals, "kv", axis=0, tiled=True),
     )
     values = lax.all_gather(values, "kv", axis=0, tiled=True)

time: 323 us -> 304 us (0.941)
  blocking collectives: 131 us -> 101 us
  waiting for transfers between devices: 83.6 us -> 90.3 us
  starting transfers between devices: 0.12 us -> 3.73 us
    all_gather x1 -> x0, blocking collectives: 30.7 us -> none  [local(): lax.all_gather(maxima, 'kv', axis=0, tiled=True)]
    all_gather x1, waiting for transfers between devices: 0.02 us -> 7.29 us  [local(): values = lax.all_gather(values, 'kv', axis=0, tiled=True)]
    all_to_all x0 -> x1, starting transfers between devices: none -> 3.62 us  [local(): lax.all_to_all(jnp.stack([maxima] * lax.axis_size('kv')), 'kv', 0, 0)]
  transfers between devices with their start and end apart: 3 -> 4, of which waited for: 2 -> 3; matrix products, arithmetic and copies ran while one was open for 3% -> 3% of each run, Pallas kernels for 0% -> 0%
where the time goes in v1:
time: 304 us; the launch traced here: 303 us
  blocking collectives  101 us (33%)
  waiting for transfers between devices  90.3 us (30%)
  matrix products  66.4 us (22%)
  other arithmetic  18.6 us (6%)
  between operations  14.7 us (5%)
  local copies, waits for them, and re-layouts  8.52 us (3%)
  starting transfers between devices  3.73 us (1%)
    psum x1, waiting for transfers between devices, local(): lax.psum((squares, query_segment, key_segment), 'kv')  51.6 us
    all_gather x1, blocking collectives, local(): lax.all_gather(totals, 'kv', axis=0, tiled=True)  31.7 us
    psum x1, waiting for transfers between devices, local(): mixed_raw = lax.psum(head_terms, 'tp')  31.3 us
    dot_general x1, matrix products, local(): jnp.einsum('snj,sja->sna', onehot.astype(jnp.bfloat16), fresh_block, pref...  25.2 us
    psum x1, blocking collectives, local(): lax.psum((squares, query_segment, key_segment), 'kv')  22.2 us
    psum x1, blocking collectives, local(): total_sq = lax.psum(jnp.sum(mixed_raw * mixed_raw, axis=-1), 'kv')  21.4 us
    dot_general x1, matrix products, partial_attend(): jnp.einsum('siha,sna->sihn', queries, key_rows, preferred_element_type=jn...  15.5 us
    dot_general x1, matrix products, partial_attend(): jnp.einsum('sihn,snk->sihk', weights.astype(jnp.bfloat16), key_rows[:, :,...  15.1 us
  transfers between devices with their start and end apart: 4, of which 3 were waited for; matrix products, arithmetic and copies ran while one was open for 3% of the time, Pallas kernels for 0%

profile of v1, /device:TPU:0, one launch (start us, length us, event | category | flops | bytes accessed | tf_op | source)
XLA Modules:
  0.0 303.5 jit_solution(15356109101237173642)
XLA Ops:
  7.2 1.3 dynamic-slice
  9.2 0.9 dynamic-update-slice
  10.1 8.4 %all-reduce = bf16[256]{0:T(256)(128)(2,1)S(1)} all-reduce(bf16[256]{0:T(256)(128)(2,1)S(1)} %dynamic-update-slice), channel_id=1, replica_groups=mesh['kv'=8,'tp'=4] {'tp'}, use_global_device_ids=true, to_apply=%add | all-reduce | flops 256 | bytes 1024
  18.5 5.8 %all_gather.18 = bf16[384,256]{0,1:T(8,128)(2,1)S(1)} all-gather(bf16[384,64]{0,1:T(8,128)(2,1)} %param.14), channel_id=1, replica_groups=mesh['kv'=8,'tp'=4] {'tp'}, dimensions={1}, use_global_device_ids=true | all-gather | bytes 245760 | tf_op jit(solution)/shard_map/all_gather | solution.py:117
  24.3 6.0 %all_gather.20 = bf16[256,512]{1,0:T(8,128)(2,1)S(1)} all-gather(bf16[64,512]{1,0:T(8,128)(2,1)} %param.19), channel_id=1, replica_groups=mesh['kv'=8,'tp'=4] {'tp'}, dimensions={0}, use_global_device_ids=true | all-gather | bytes 327680 | tf_op jit(solution)/shard_map/all_gather | solution.py:119
  30.3 5.8 %all_gather.21 = bf16[256,288]{1,0:T(8,128)(2,1)S(1)} all-gather(bf16[64,288]{1,0:T(8,128)(2,1)} %param.20), channel_id=1, replica_groups=mesh['kv'=8,'tp'=4] {'tp'}, dimensions={0}, use_global_device_ids=true | all-gather | bytes 184320 | tf_op jit(solution)/shard_map/all_gather | solution.py:120
  36.1 1.3 fusion.49
  37.4 1.1 fusion.47
  38.6 22.2 %psum.36 = f32[384]{0:T(512)S(1)} all-reduce(f32[384]{0:T(512)S(1)} %fusion.28), channel_id=1, replica_groups=mesh['kv'=8,'tp'=4] {'kv'}, use_global_device_ids=true, to_apply=%region_2.0 | all-reduce | flops 384 | bytes 3072 | tf_op jit(solution)/shard_map/psum | solution.py:123
  61.5 0.8 copy.38
  65.4 1.5 fusion.12
  67.0 2.0 compare_or_fusion
  69.1 51.6 %all-reduce.7.cloned.1.call-done = (f32[384,288]{0,1:T(8,128)}, f32[384,512]{1,0:T(8,128)}) async-done(((f32[384,288]{0,1:T(8,128)}, f32[384,512]{1,0:T(8,128)}), (f32[384,288]{0,1:T(8,128)}, f32[384,512]{1,0:T(8,128)})) %all-reduce.7.cloned.1.call-update) | async-done | bytes 1228816 | tf_op jit(solution)/shard_map/psum | solution.py:123
  120.7 1.0 broadcast_multiply_fusion
  123.0 0.7 copy.62
  123.7 1.4 multiply_reduce_fusion.1
  125.1 2.0 fusion.22
  128.9 25.2 %convert_select_fusion = bf16[24,2048,288]{1,2,0:T(8,128)(2,1)} fusion(bf16[24,2048,288]{1,2,0:T(8,128)(2,1)} %param.15, pred[24,2048]{1,0:T(8,128)(4,1)} %fusion.12, s32[24,2048]{1,0:T(8,128)S(1)} %broadcast_subtract_fusion, bf16[24,16,16]{2,1,0:T(8,128)(2,1)} %bitcast.69, bf16[24,16,16]{2,1,0:T(8,128)(2,1)} %bitcast.68, bf16[24,16,256]{2,1,0:T(8,128)(2,1)S(1)} %bitcast.67), kind=kOutput, calls=%fused_computation.2 | convolution fusion | flops 482746368 | bytes 57090048 | tf_op jit(solution)/shard_map/snj,sja->sna/dot_general | solution.py:141
  154.1 15.5 %fusion.3 = (f32[24,16,4]{1,2,0:T(4,128)S(1)}, f32[24,16,4,2048]{3,1,2,0:T(8,128)}) fusion(pred[24,16,2048]{2,1,0:T(8,128)(4,1)S(1)} %compare_or_fusion, bf16[24,2048,288]{1,2,0:T(8,128)(2,1)} %convert_select_fusion, bf16[24,16,4,16]{3,1,2,0:T(8,128)(2,1)S(1)} %copy.44, bf16[24,16,4,16]{3,1,2,0:T(8,128)(2,1)S(1)} %copy.43, ...), kind=kOutput, calls=%fused_computation.7 | convolution fusion | flops 1824029184 | bytes 42571776 | tf_op jit(solution)/shard_map/siha,sna->sihn/dot_general | solution.py:65
  169.6 6.9 %fusion.5 = f32[24,16,4]{1,2,0:T(4,128)S(1)} fusion(f32[24,16,4,2048]{3,1,2,0:T(8,128)} %get-tuple-element.17, f32[24,16,4]{1,2,0:T(4,128)S(1)} %get-tuple-element.16, pred[24,16,2048]{2,1,0:T(8,128)(4,1)S(1)} %compare_or_fusion), kind=kLoop, calls=%fused_computation.9 | loop fusion | flops 15727104 | bytes 13381632 | tf_op jit(solution)/shard_map/reduce_sum | solution.py:71
  176.5 15.1 %divide_convert_fusion = bf16[24,16,4,256]{3,1,2,0:T(8,128)(2,1)S(1)} fusion(bf16[24,2048,288]{1,2,0:T(8,128)(2,1)} %convert_select_fusion, f32[24,16,4,2048]{3,1,2,0:T(8,128)} %get-tuple-element.17, f32[24,16,4]{1,2,0:T(4,128)S(1)} %get-tuple-element.16, pred[24,16,2048]{2,1,0:T(8,128)(4,1)S(1)} %compare_or_fusion, f32[24,16,4]{1,2,0:T(4,128)S(1)} %broadcast_maximum_fusion), kind=kOutput, calls=%fused_computation.21 | convolution fusion | flops 1627127808 | bytes 39333888 | tf_op jit(solution)/shard_map/sihn,snk->sihk/dot_general | solution.py:72
  191.7 1.6 fusion.16
  193.4 0.8 copy.53
  195.0 3.6 %all-to-all-start = ((f32[8,1,384,4]{2,3,1,0:T(4,128)}), f32[8,1,384,4]{2,3,1,0:T(4,128)S(1)}, u32[]{:S(2)}, u32[]{:S(2)}) async-start(f32[8,1,384,4]{2,3,1,0:T(4,128)} %stack.3), calls=%async_computation | async-start | bytes 98304 | tf_op jit(solution)/shard_map/all_to_all | solution.py:161
  198.7 31.7 %all_gather.22 = f32[8,384,4]{1,2,0:T(4,128)S(1)} all-gather(f32[1,384,4]{1,2,0:T(4,128)S(1)} %reshape.203), channel_id=1, replica_groups=mesh['kv'=8,'tp'=4] {'kv'}, dimensions={0}, use_global_device_ids=true | all-gather | bytes 55296 | tf_op jit(solution)/shard_map/all_gather | solution.py:163
  230.4 7.3 %all-gather.2.cloned.1.call-done = bf16[8,384,4,64]{1,3,2,0:T(8,128)(2,1)} async-done(((bf16[1,384,4,64]{1,3,2,0:T(8,128)(2,1)}), bf16[8,384,4,64]{1,3,2,0:T(8,128)(2,1)}) %all-gather.2.cloned.1.call-update) | async-done | bytes 1572880 | tf_op jit(solution)/shard_map/all_gather | solution.py:165
  237.7 1.8 multiply_reduce_fusion
  240.3 1.0 fusion.64
  241.3 31.3 %all-reduce.5.cloned.1.call-done = f32[384,256]{1,0:T(8,128)} async-done(((f32[384,256]{1,0:T(8,128)}), f32[384,256]{1,0:T(8,128)}) %all-reduce.5.cloned.1.call-update) | async-done | bytes 393232 | tf_op jit(solution)/shard_map/psum | solution.py:168
  272.6 1.1 multiply_reduce_fusion.2
  273.8 21.4 %psum.39 = f32[384]{0:T(512)S(1)} all-reduce(f32[384]{0:T(512)S(1)} %multiply_reduce_fusion.2), channel_id=1, replica_groups=mesh['kv'=8,'tp'=4] {'kv'}, use_global_device_ids=true, to_apply=%region_15.16 | all-reduce | flops 384 | bytes 3072 | tf_op jit(solution)/shard_map/psum | solution.py:169
  295.1 1.8 multiply_convert_fusion.1
  (61 shorter events, 8.8 us)
Async XLA Ops:
  7.2 117.9 %copy-start = (bf16[512,4,288]{0,2,1:T(8,128)(2,1)S(1)}, bf16[512,4,288]{0,2,1:T(8,128)(2,1)}, u32[]{:S(2)}) copy-start(bf16[512,4,288]{0,2,1:T(8,128)(2,1)} %param.24) | copy-start | bytes 3538948
  7.2 113.5 %all-reduce.7.cloned.1.call-start = ((), (), s32[]{:S(2)}) async-start(), calls=%async_computation.3 | async-start | bytes 2457600 | tf_op jit(solution)/shard_map/psum | solution.py:123
  38.5 199.2 %all-gather.2.cloned.1.call-start = ((), (), s32[]{:S(2)}) async-start(), calls=%async_computation.1 | async-start | bytes 1769472 | tf_op jit(solution)/shard_map/all_gather | solution.py:165
  176.5 63.7 %copy-start.2 = (bf16[256,256]{1,0:T(8,128)(2,1)S(1)}, bf16[256,256]{1,0:T(8,128)(2,1)}, u32[]{:S(2)}) copy-start(bf16[256,256]{1,0:T(8,128)(2,1)} %param.26) | copy-start | bytes 393220
  176.5 64.8 %copy-start.3 = (bf16[256]{0:T(256)(128)(2,1)S(1)}, bf16[256]{0:T(256)(128)(2,1)}, u32[]{:S(2)}) copy-start(bf16[256]{0:T(256)(128)(2,1)} %param.27) | copy-start | bytes 1540
  176.5 120.4 %copy-start.1 = (bf16[512,4,288]{0,2,1:T(8,128)(2,1)S(1)}, bf16[512,4,288]{0,2,1:T(8,128)(2,1)}, u32[]{:S(2)}) copy-start(bf16[512,4,288]{0,2,1:T(8,128)(2,1)} %param.24) | copy-start | bytes 3538948
  195.0 35.4 %all-to-all-start = ((f32[8,1,384,4]{2,3,1,0:T(4,128)}), f32[8,1,384,4]{2,3,1,0:T(4,128)S(1)}, u32[]{:S(2)}, u32[]{:S(2)}) async-start(f32[8,1,384,4]{2,3,1,0:T(4,128)} %stack.3), calls=%async_computation | async-start | bytes 98304 | tf_op jit(solution)/shard_map/all_to_all | solution.py:161
  198.6 74.1 %all-reduce.5.cloned.1.call-start = ((), (), s32[]{:S(2)}) async-start(), calls=%async_computation.2 | async-start | bytes 786432 | tf_op jit(solution)/shard_map/psum | solution.py:168
Sparse Core Ops, SparseCore 0:
  38.6 81.9 all-reduce.6
  194.4 43.3 all-gather.1
  241.4 31.1 all-reduce.4
